TPU v7x, 32 devices: a whole 2x2x4 slice. The times are simulated.
32 devices in a mesh: rep: 4 (over z), fs: 4 (over y, x), tp: 2 (over core).
Axes of the slice: x: 2, y: 2, z: 4, core: 2. Of those that a mesh axis runs over, the one named last changes fastest.
Arguments:
- gate_pre: bfloat16 [2560, 2816], P(('rep', 'fs'), 'tp'), may hold values from -6 to 6
- up_pre: bfloat16 [2560, 2816], P(('rep', 'fs'), 'tp'), may hold values from -6 to 6
- gate_taps: bfloat16 [3, 2816], P(None, 'tp'), may hold values from -3 to 3
- up_taps: bfloat16 [3, 2816], P(None, 'tp'), may hold values from -3 to 3
- down_weight: bfloat16 [2816, 2048], P('tp', 'fs'), may hold values from -0.125 to 0.125
- cotangent: bfloat16 [2560, 2048], P('rep', 'fs'), may hold values from -6 to 6
Outputs:
- grad_gate: bfloat16 [2560, 2816], P(('rep', 'fs'), 'tp')
- grad_up: bfloat16 [2560, 2816], P(('rep', 'fs'), 'tp')
- grad_gate_taps: float32 [3, 2816], P(None, 'tp')
- grad_up_taps: float32 [3, 2816], P(None, 'tp')
- grad_down: float32 [4, 512, 2816], P('fs', 'rep', 'tp')
- down_norms: float32 [2816], P('tp')
All inputs are finite; a program needn't handle non-finite values.
Results may differ from a plain program's by a relative error of at most 0.0049.
Values may be sent and summed in bfloat16 or wider, within the bound.
A program may use at most 64 MiB of HBM per device.

v0:
```python
import jax
import jax.numpy as jnp
from jax import lax
from jax.sharding import PartitionSpec as P

D = 2048


def passed_along(array, axis, by):
    count = lax.axis_size(axis)
    pairs = [(i, i + by) for i in range(count) if 0 <= i + by < count]
    return lax.ppermute(array, axis, pairs)


def shift_conv(padded, tap_coef):
    return tap_coef[0] * padded[:-2] + tap_coef[1] * padded[1:-1] + tap_coef[2] * padded[2:]


def back_conv(padded, tap_coef):
    return tap_coef[2] * padded[:-2] + tap_coef[1] * padded[1:-1] + tap_coef[0] * padded[2:]


def local(gate_pre, up_pre, gate_taps, up_taps, down_weight, cotangent):
    tok_rows = gate_pre.shape[0]
    width = gate_pre.shape[1]
    prev_rows = passed_along(jnp.stack([gate_pre[-2:], up_pre[-2:]]), "fs", 1)
    gate_pad = jnp.concatenate([prev_rows[0], gate_pre], 0).astype(jnp.float32)
    up_pad = jnp.concatenate([prev_rows[1], up_pre], 0).astype(jnp.float32)
    gate_coef = gate_taps.astype(jnp.float32)
    up_coef = up_taps.astype(jnp.float32)
    gate_conv = shift_conv(gate_pad, gate_coef)
    up_conv = shift_conv(up_pad, up_coef)
    gate_sig = jax.nn.sigmoid(gate_conv)
    activated = gate_conv * gate_sig
    hidden = (activated * up_conv).astype(jnp.bfloat16)
    partial_rows = lax.dot_general(
        cotangent, down_weight, (((1,), (1,)), ((), ())), preferred_element_type=jnp.float32
    ).astype(jnp.bfloat16)
    received = lax.all_to_all(partial_rows, "fs", split_axis=0, concat_axis=0, tiled=True)
    d_hidden = jnp.sum(received.reshape(-1, tok_rows, width).astype(jnp.float32), axis=0)
    d_gate = d_hidden * up_conv * gate_sig * (1.0 + gate_conv * (1.0 - gate_sig))
    d_up = d_hidden * activated
    next_rows = passed_along(jnp.stack([d_gate[:2], d_up[:2]]), "fs", -1)
    grad_gate = back_conv(jnp.concatenate([d_gate, next_rows[0]], 0), gate_coef).astype(
        jnp.bfloat16
    )
    grad_up = back_conv(jnp.concatenate([d_up, next_rows[1]], 0), up_coef).astype(jnp.bfloat16)
    taps_part = jnp.stack(
        [
            jnp.stack(
                [
                    jnp.sum(d_gate * gate_pad[offset : offset + tok_rows], axis=0)
                    for offset in range(3)
                ]
            ),
            jnp.stack(
                [jnp.sum(d_up * up_pad[offset : offset + tok_rows], axis=0) for offset in range(3)]
            ),
        ]
    )
    grad_scale = float(tok_rows * lax.axis_size("rep") * lax.axis_size("fs")) ** (-0.5)
    folded_sum = lax.dot_general(
        cotangent,
        lax.all_gather(hidden, "fs", axis=0, tiled=True),
        (((0,), (0,)), ((), ())),
        preferred_element_type=jnp.float32,
    )
    grad_share = lax.psum_scatter(folded_sum, "rep", scatter_dimension=0, tiled=True)
    grad_share = grad_share * grad_scale
    norm_part = jnp.sum(grad_share * grad_share, axis=0)
    norm_total, taps_total = lax.psum((norm_part, taps_part), ("rep", "fs"))
    return (
        grad_gate,
        grad_up,
        taps_total[0] * grad_scale,
        taps_total[1] * grad_scale,
        grad_share[None],
        norm_total / D,
    )


def solution(mesh):
    return jax.shard_map(
        local,
        mesh=mesh,
        in_specs=(
            P(("rep", "fs"), "tp"),
            P(("rep", "fs"), "tp"),
            P(None, "tp"),
            P(None, "tp"),
            P("tp", "fs"),
            P("rep", "fs"),
        ),
        out_specs=(
            P(("rep", "fs"), "tp"),
            P(("rep", "fs"), "tp"),
            P(None, "tp"),
            P(None, "tp"),
            P("fs", "rep", "tp"),
            P("tp"),
        ),
        check_vma=False,
    )
```

profile of v0, /device:TPU:0, one launch (start us, length us, event | category | flops | bytes accessed | tf_op | source)
XLA Modules:
  0.0 199.6 jit_solution(9646430409781421393)
XLA Ops:
  7.2 0.0 copy-start
  7.2 0.0 all-gather.2.cloned.1.call-start
  7.2 0.9 slice_bitcast_fusion.6
  8.2 4.9 %collective-permute-start = (bf16[2,2,1408]{2,1,0:T(2,128)(2,1)S(1)}, bf16[2,2,1408]{2,1,0:T(2,128)(2,1)S(1)}, u32[]{:S(2)}, u32[]{:S(2)}) collective-permute-start(bf16[2,2,1408]{2,1,0:T(2,128)(2,1)S(1)} %pad_maximum_fusion.4), channel_id=1, source_target_pairs={{0,2},{2,4},{4,6},{1,3},{3,5},{5,7},{8,10},{10,12},{12,14},{9,11},... | collective-permute-start | bytes 33800 | tf_op jit(solution)/shard_map/ppermute | solution.py:12
  13.0 0.7 convert_element_type.27
  13.8 0.7 convert_element_type.30
  14.5 0.1 slice_reduce_fusion.4
  14.6 0.0 collective-permute-done
  14.6 1.1 maximum_convert_fusion
  15.7 0.1 maximum_convert_fusion.1
  15.8 1.8 multiply_convert_fusion
  17.6 0.0 all-gather.2.cloned.1.call-update
  17.6 0.0 reduce-scatter.2.cloned.1.call-start
  17.7 34.7 %all-gather.2.cloned.1.call-done = bf16[640,1408]{1,0:T(8,128)(2,1)} async-done(((bf16[160,1408]{1,0:T(8,128)(2,1)}), bf16[640,1408]{1,0:T(8,128)(2,1)}) %all-gather.2.cloned.1.call-update) | async-done | bytes 1802256 | tf_op jit(solution)/shard_map/all_gather | solution.py:64
  52.4 4.5 %convolution_bitcast_fusion = f32[512,1408]{0,1:T(8,128)} fusion(bf16[640,1408]{1,0:T(8,128)(2,1)} %all-gather.2.cloned.1.call-done, bf16[640,512]{1,0:T(8,128)(2,1)} %param.11), kind=kOutput, calls=%fused_computation.1 | convolution fusion | flops 922746880 | bytes 5341184 | tf_op jit(solution)/shard_map/dot_general | solution.py:62
  56.9 0.0 reduce-scatter.2.cloned.1.call-update
  57.0 2.3 %convolution_convert_fusion = bf16[640,1408]{1,0:T(8,128)(2,1)S(1)} fusion(bf16[640,512]{1,0:T(8,128)(2,1)} %param.11, bf16[1408,512]{1,0:T(8,128)(2,1)S(1)} %copy-done), kind=kOutput, calls=%fused_computation.2 | convolution fusion | flops 923648000 | bytes 3899392 | tf_op jit(solution)/shard_map/dot_general | solution.py:36
  59.3 24.9 %all_to_all.9 = bf16[4,160,1408]{2,1,0:T(8,128)(2,1)S(1)} all-to-all(bf16[4,160,1408]{2,1,0:T(8,128)(2,1)S(1)} %bitcast.33), channel_id=1, replica_groups=mesh['rep'=4,'fs'=4,'tp'=2] {'fs'}, dimensions={0} | all-to-all | bytes 3604480 | tf_op jit(solution)/shard_map/all_to_all | solution.py:39
  84.1 0.2 convert_reduce_fusion
  84.4 0.9 copy-done.1
  85.3 0.3 copy-done.2
  85.6 1.1 multiply_reduce_fusion.2
  86.8 1.3 collective-permute-start.1
  88.2 4.3 %collective-permute-done.1 = f32[2,2,1408]{2,1,0:T(2,128)S(1)} collective-permute-done((f32[2,2,1408]{2,1,0:T(2,128)S(1)}, f32[2,2,1408]{2,1,0:T(2,128)S(1)}, u32[]{:S(2)}, u32[]{:S(2)}) %collective-permute-start.1) | collective-permute-done | bytes 22560 | tf_op jit(solution)/shard_map/ppermute | solution.py:12
  92.5 1.1 fusion.9
  93.5 1.1 fusion.4
  94.6 18.8 %reduce-scatter.2.cloned.1.call-done = f32[128,1408]{0,1:T(8,128)} async-done(((f32[512,1408]{0,1:T(8,128)}), f32[128,1408]{0,1:T(8,128)}) %reduce-scatter.2.cloned.1.call-update) | async-done | bytes 720912 | tf_op jit(solution)/shard_map/reduce_scatter | solution.py:68
  113.4 1.4 multiply_bitcast_fusion
  114.8 1.1 copy.12
  116.0 75.6 %all-reduce = (f32[2,3,1408]{2,1,0:T(4,128)S(1)}, f32[1408]{0:T(1024)S(1)}) all-reduce(f32[2,3,1408]{2,1,0:T(4,128)S(1)} %pad_maximum_fusion.2, f32[1408]{0:T(1024)S(1)} %get-tuple-element.36), channel_id=1, replica_groups=mesh['rep'=4,'fs'=4,'tp'=2] {'rep','fs'}, use_global_device_ids=true, to_apply=%region_7.0 | all-reduce | flops 9856 | bytes 78848 | tf_op jit(solution)/shard_map/psum | solution.py:71
  191.5 0.6 fusion.14
  192.2 0.6 broadcast_multiply_fusion
  (20 shorter events, 0.2 us)
Async XLA Ops:
  7.2 49.8 %copy-start = (bf16[1408,512]{1,0:T(8,128)(2,1)S(1)}, bf16[1408,512]{1,0:T(8,128)(2,1)}, u32[]{:S(2)}) copy-start(bf16[1408,512]{1,0:T(8,128)(2,1)} %param.10) | copy-start | bytes 4325380
  7.2 45.2 %all-gather.2.cloned.1.call-start = ((), (), s32[]{:S(2)}) async-start(), calls=%async_computation.2 | async-start | bytes 2252800 | tf_op jit(solution)/shard_map/all_gather | solution.py:64
  7.2 8.5 %copy-start.3 = (bf16[160,1408]{1,0:T(8,128)(2,1)S(1)}, bf16[160,1408]{1,0:T(8,128)(2,1)}, u32[]{:S(2)}) copy-start(bf16[160,1408]{1,0:T(8,128)(2,1)} %param.6) | copy-start | bytes 1351684
  8.2 6.4 %collective-permute-start = (bf16[2,2,1408]{2,1,0:T(2,128)(2,1)S(1)}, bf16[2,2,1408]{2,1,0:T(2,128)(2,1)S(1)}, u32[]{:S(2)}, u32[]{:S(2)}) collective-permute-start(bf16[2,2,1408]{2,1,0:T(2,128)(2,1)S(1)} %pad_maximum_fusion.4), channel_id=1, source_target_pairs={{0,2},{2,4},{4,6},{1,3},{3,5},{5,7},{8,10},{10,12},{12,14},{9,11},... | collective-permute-start | bytes 33800 | tf_op jit(solution)/shard_map/ppermute | solution.py:12
  17.6 95.8 %reduce-scatter.2.cloned.1.call-start = ((), (), s32[]{:S(2)}) async-start(), calls=%async_computation.3 | async-start | bytes 3604480 | tf_op jit(solution)/shard_map/reduce_scatter | solution.py:68
  84.1 1.2 copy-start.1
  84.1 1.4 copy-start.2
  86.8 5.7 %collective-permute-start.1 = (f32[2,2,1408]{2,1,0:T(2,128)S(1)}, f32[2,2,1408]{2,1,0:T(2,128)S(1)}, u32[]{:S(2)}, u32[]{:S(2)}) collective-permute-start(f32[2,2,1408]{2,1,0:T(2,128)S(1)} %pad_maximum_fusion.3), channel_id=1, source_target_pairs={{2,0},{4,2},{6,4},{3,1},{5,3},{7,5},{10,8},{12,10},{14,12},{11,9},... | collective-permute-start | bytes 67592 | tf_op jit(solution)/shard_map/ppermute | solution.py:12
Sparse Core Ops, SparseCore 0:
  17.7 34.6 all-gather.1
  57.1 56.3 reduce-scatter.1
where the time goes:
time: 200 us
  blocking collectives  100 us (50%)
  waiting for transfers between devices  57.9 us (29%)
  between operations  14.2 us (7%)
  other arithmetic  10.6 us (5%)
  matrix products  6.82 us (3%)
  starting transfers between devices  6.24 us (3%)
  local copies, waits for them, and re-layouts  3.38 us (2%)
    psum x1, blocking collectives, local(): norm_total, taps_total = lax.psum((norm_part, taps_part), ('rep', 'fs'))  75.6 us
    all_gather x1, waiting for transfers between devices, local(): lax.all_gather(hidden, 'fs', axis=0, tiled=True)  34.7 us
    all_to_all x1, blocking collectives, local(): lax.all_to_all(partial_rows, 'fs', split_axis=0, concat_axis=0, tiled=True)  24.9 us
    reduce_scatter x1, waiting for transfers between devices, local(): lax.psum_scatter(folded_sum, 'rep', scatter_dimension=0, tiled=True)  18.8 us
    ppermute x2, starting transfers between devices, passed_along(): return lax.ppermute(array, axis, pairs)  6.16 us
    dot_general x1, matrix products, local(): lax.dot_general(cotangent, lax.all_gather(hidden, 'fs', axis=0, tiled=Tru...  4.52 us
    ppermute x2, waiting for transfers between devices, passed_along(): return lax.ppermute(array, axis, pairs)  4.32 us
  transfers between devices with their start and end apart: 4, of which 3 were waited for; matrix products, arithmetic and copies ran while one was open for 4% of the time, Pallas kernels for 0%

commit v1 on v0

--- a/solution.py
+++ b/solution.py
@@ -1,9 +1,14 @@
+import functools
+
 import jax
 import jax.numpy as jnp
 from jax import lax
+from jax.experimental import pallas as pl
+from jax.experimental.pallas import tpu as pltpu
 from jax.sharding import PartitionSpec as P
 
-D = 2048
+MESH = pl.DeviceIdType.MESH
+LANES = 128
 
 
 def passed_along(array, axis, by):
@@ -75,13 +80,348 @@
         taps_total[0] * grad_scale,
         taps_total[1] * grad_scale,
         grad_share[None],
-        norm_total / D,
+        norm_total / (cotangent.shape[1] * lax.axis_size("fs")),
     )
+
+
+HALO = 16
+FS_MASKS = ((1, 2), (2, 1))
+REP_MASKS = ((1, 2), (1, 2))
+
+
+def flip(v, mask):
+    if mask == 1:
+        return v + 1 - 2 * (v % 2)
+    if mask == 2:
+        return (v + 2) % 4
+    return 3 - v
+
+
+def column_chunks(width):
+    tiles = width // LANES
+    widths = [1, 1, 2, 2]
+    rest = tiles - sum(widths)
+    if rest < 2:
+        widths, rest = [], tiles
+    widths = widths + [rest // 2, rest - rest // 2] if rest > 1 else [rest]
+    chunks, at = [], 0
+    for tiles_here in widths:
+        chunks.append((at * LANES, tiles_here * LANES))
+        at += tiles_here
+    return chunks
+
+
+def kernel(
+    scale, model_width, gate_hbm, up_hbm, gtaps_hbm, utaps_hbm, weight_hbm, cot_hbm,
+    grad_gate, grad_up, gtaps_out, utaps_out, grad_down, norms_out,
+    gate, up, gtaps, utaps, weight, cot, cot_t, halo, gate_pad, up_pad, coef_gate, coef_up,
+    hid, parts, rs1, rs2, rs_out, prod, prod_out, zs1, zs2, z_out, dg_pad, du_pad,
+    dhalo_out, dhalo_in, taps_out1, taps_in1, taps_out2, taps_in2,
+    norm_out1, norm_in1, norm_out2, norm_in2, load_sem, send_sem, recv_sem,
+):
+    f = lax.axis_index("fs")
+    r = lax.axis_index("rep")
+    rows, width = gate.shape
+    blk = grad_down.shape[0]
+    chunks = column_chunks(width)
+    n = len(chunks)
+    sends = []
+
+    loads = []
+    for i, (src, dst) in enumerate((
+        (gate_hbm, gate), (up_hbm, up), (cot_hbm, cot), (weight_hbm, weight),
+        (gtaps_hbm, gtaps), (utaps_hbm, utaps),
+    )):
+        copy = pltpu.make_async_copy(src, dst, load_sem.at[i])
+        copy.start()
+        loads.append(copy)
+
+    barrier = pltpu.get_barrier_semaphore()
+    for d in (1, 2, 3):
+        pl.semaphore_signal(barrier, inc=1, device_id={"fs": (f + d) % 4}, device_id_type=MESH)
+        pl.semaphore_signal(barrier, inc=1, device_id={"rep": (r + d) % 4}, device_id_type=MESH)
+    pl.semaphore_wait(barrier, 6)
+
+    def push(src, dst, axis, to):
+        k = len(sends)
+        copy = pltpu.make_async_remote_copy(
+            src_ref=src, dst_ref=dst, send_sem=send_sem.at[k], recv_sem=recv_sem.at[k],
+            device_id={axis: to}, device_id_type=MESH,
+        )
+        copy.start()
+        sends.append(copy)
+        return copy
+
+    def cols(c):
+        return pl.ds(chunks[c][0], chunks[c][1])
+
+    def tile_list(c):
+        return [pl.ds(at, LANES) for at in range(chunks[c][0], chunks[c][0] + chunks[c][1], LANES)]
+
+    loads[0].wait()
+    loads[1].wait()
+    nxt = (f + 1) % 4
+    halo_in = [
+        push(gate.at[pl.ds(rows - HALO, HALO)], halo.at[0], "fs", nxt),
+        push(up.at[pl.ds(rows - HALO, HALO)], halo.at[1], "fs", nxt),
+    ]
+
+    def part(c):
+        product = lax.dot_general(
+            cot[...], weight[cols(c), :], (((1,), (1,)), ((), ())),
+            preferred_element_type=jnp.float32,
+        )
+        parts[:, :, cols(c)] = product.astype(jnp.bfloat16).reshape(4, rows, chunks[c][1])
+
+    rs1_in, rs2_in, ag1_in, ag2_in, z1_in, z2_in = {}, {}, {}, {}, {}, {}
+
+    def rs_first(c):
+        m1, m2 = FS_MASKS[c % 2]
+        to = flip(f, m1)
+        rs1_in[c] = [
+            push(parts.at[flip(to, m2), :, cols(c)], rs1.at[1, :, cols(c)], "fs", to),
+            push(parts.at[to, :, cols(c)], rs1.at[0, :, cols(c)], "fs", to),
+        ]
+
+    def rs_second(c):
+        m1, m2 = FS_MASKS[c % 2]
+        to = flip(f, m2)
+        rs1_in[c][0].wait_recv()
+        for t in tile_list(c):
+            rs_out[:, t] = (
+                parts[to, :, t].astype(jnp.float32) + rs1[1, :, t].astype(jnp.float32)
+            ).astype(jnp.bfloat16)
+        rs2_in[c] = push(rs_out.at[:, cols(c)], rs2.at[:, cols(c)], "fs", to)
+
+    def hidden(c):
+        for t in tile_list(c):
+            gc = [gtaps[k : k + 1, t].astype(jnp.float32) for k in range(3)]
+            uc = [utaps[k : k + 1, t].astype(jnp.float32) for k in range(3)]
+            g_conv = sum(gc[k] * gate_pad[pl.ds(6 + k, rows), t] for k in range(3))
+            u_conv = sum(uc[k] * up_pad[pl.ds(6 + k, rows), t] for k in range(3))
+            sig = jax.nn.sigmoid(g_conv)
+            act = g_conv * sig
+            hid[f, :, t] = (act * u_conv).astype(jnp.bfloat16)
+            coef_up[:, t] = act
+            coef_gate[:, t] = u_conv * sig * (1.0 + g_conv * (1.0 - sig))
+        m1, m2 = FS_MASKS[c % 2]
+        ag1_in[c] = push(hid.at[f, :, cols(c)], hid.at[f, :, cols(c)], "fs", flip(f, m1))
+
+    def ag_second(c):
+        m1, m2 = FS_MASKS[c % 2]
+        to = flip(f, m2)
+        own = push(hid.at[f, :, cols(c)], hid.at[f, :, cols(c)], "fs", to)
+        ag1_in[c].wait_recv()
+        slot = flip(f, m1)
+        ag2_in[c] = [own, push(hid.at[slot, :, cols(c)], hid.at[slot, :, cols(c)], "fs", to)]
+
+    def product(c):
+        for copy in ag2_in[c]:
+            copy.wait_recv()
+        result = jnp.dot(
+            cot_t[...], hid[:, :, cols(c)].reshape(4 * rows, chunks[c][1]),
+            preferred_element_type=jnp.float32,
+        ).reshape(4, blk, chunks[c][1])
+        prod[:, :, cols(c)] = result
+        prod_out[:, :, cols(c)] = result.astype(jnp.bfloat16)
+        m1, m2 = REP_MASKS[c % 2]
+        to = flip(r, m1)
+        z1_in[c] = [
+            push(prod_out.at[flip(to, m2), :, cols(c)], zs1.at[1, :, cols(c)], "rep", to),
+            push(prod_out.at[to, :, cols(c)], zs1.at[0, :, cols(c)], "rep", to),
+        ]
+
+    def z_second(c):
+        m1, m2 = REP_MASKS[c % 2]
+        to = flip(r, m2)
+        z1_in[c][0].wait_recv()
+        for t in tile_list(c):
+            z_out[:, t] = (prod[to, :, t] + zs1[1, :, t].astype(jnp.float32)).astype(jnp.bfloat16)
+        z2_in[c] = push(z_out.at[:, cols(c)], zs2.at[:, cols(c)], "rep", to)
+
+    def z_last(c):
+        z1_in[c][1].wait_recv()
+        z2_in[c].wait_recv()
+        for t in tile_list(c):
+            total = (
+                prod[r, :, t] + zs1[0, :, t].astype(jnp.float32) + zs2[:, t].astype(jnp.float32)
+            ) * scale
+            grad_down[:, t] = total
+            norm_out1[:, t] = jnp.sum(total * total, axis=0, keepdims=True)
+
+    def rs_last(c):
+        rs1_in[c][1].wait_recv()
+        rs2_in[c].wait_recv()
+        for t in tile_list(c):
+            dh = (
+                parts[f, :, t].astype(jnp.float32)
+                + rs1[0, :, t].astype(jnp.float32)
+                + rs2[:, t].astype(jnp.float32)
+            )
+            d_gate = dh * coef_gate[:, t]
+            d_up = dh * coef_up[:, t]
+            dg_pad[pl.ds(0, rows), t] = d_gate
+            du_pad[pl.ds(0, rows), t] = d_up
+            dhalo_out[0:2, t] = d_gate[0:2]
+            dhalo_out[2:4, t] = d_up[0:2]
+            for k in range(3):
+                taps_out1[k : k + 1, t] = jnp.sum(
+                    d_gate * gate_pad[pl.ds(6 + k, rows), t], axis=0, keepdims=True
+                )
+                taps_out1[3 + k : 4 + k, t] = jnp.sum(
+                    d_up * up_pad[pl.ds(6 + k, rows), t], axis=0, keepdims=True
+                )
+
+    def spread(src, landing, axis, me):
+        return [push(src, landing.at[me], axis, (me + d) % 4) for d in (1, 2, 3)]
+
+    def gather_sum(copies, own, landing, me):
+        for copy in copies:
+            copy.wait_recv()
+        landing[me] = own[...]
+        return (landing[0] + landing[1]) + (landing[2] + landing[3])
+
+    loads[2].wait()
+    loads[3].wait()
+    part(0)
+    rs_first(0)
+    part(1)
+    rs_first(1)
+    gate_pad[pl.ds(8, rows), :] = gate[...].astype(jnp.float32)
+    up_pad[pl.ds(8, rows), :] = up[...].astype(jnp.float32)
+    taps_out1[...] = jnp.zeros_like(taps_out1)
+    dhalo_out[...] = jnp.zeros_like(dhalo_out)
+    loads[4].wait()
+    loads[5].wait()
+    for copy in halo_in:
+        copy.wait_recv()
+    inner = (f > 0).astype(jnp.float32)
+    gate_pad[6:8, :] = halo[0].astype(jnp.float32)[HALO - 2 :] * inner
+    up_pad[6:8, :] = halo[1].astype(jnp.float32)[HALO - 2 :] * inner
+
+    hidden(0)
+    hidden(1)
+    hidden(2)
+    hidden(3)
+    ag_second(0)
+    ag_second(1)
+    cot_t[...] = cot[...].T
+    hidden(4)
+    hidden(5)
+    ag_second(2)
+    ag_second(3)
+    part(2)
+    part(3)
+    product(0)
+    product(1)
+    ag_second(4)
+    ag_second(5)
+    rs_first(2)
+    rs_first(3)
+    part(4)
+    part(5)
+    product(2)
+    product(3)
+    z_second(0)
+    z_second(1)
+    rs_second(0)
+    rs_second(1)
+    rs_first(4)
+    rs_first(5)
+    product(4)
+    product(5)
+    z_second(2)
+    z_second(3)
+    rs_second(2)
+    rs_second(3)
+    z_last(0)
+    z_last(1)
+    rs_last(0)
+    rs_last(1)
+    rs_second(4)
+    rs_second(5)
+    rs_last(2)
+    rs_last(3)
+    z_second(4)
+    z_second(5)
+    z_last(2)
+    z_last(3)
+    rs_last(4)
+    rs_last(5)
+    taps1 = spread(taps_out1, taps_in1, "fs", f)
+    dhalo = push(dhalo_out, dhalo_in, "fs", (f + 3) % 4)
+    z_last(4)
+    z_last(5)
+    norm1 = spread(norm_out1, norm_in1, "fs", f)
+    taps_out2[...] = gather_sum(taps1, taps_out1, taps_in1, f)
+    taps2 = spread(taps_out2, taps_in2, "rep", r)
+    norm_out2[...] = gather_sum(norm1, norm_out1, norm_in1, f)
+    norm2 = spread(norm_out2, norm_in2, "rep", r)
+    dhalo.wait_recv()
+    inner = (f < 3).astype(jnp.float32)
+    dg_pad[rows : rows + 2, :] = dhalo_in[0:2, :] * inner
+    du_pad[rows : rows + 2, :] = dhalo_in[2:4, :] * inner
+    for c in range(n):
+        for t in tile_list(c):
+            for taps, pad, out in ((gtaps, dg_pad, grad_gate), (utaps, du_pad, grad_up)):
+                out[:, t] = sum(
+                    taps[2 - k : 3 - k, t].astype(jnp.float32) * pad[pl.ds(k, rows), t]
+                    for k in range(3)
+                ).astype(jnp.bfloat16)
+    taps_total = gather_sum(taps2, taps_out2, taps_in2, r) * scale
+    gtaps_out[...] = taps_total[0:3]
+    utaps_out[...] = taps_total[3:6]
+    norms_out[...] = gather_sum(norm2, norm_out2, norm_in2, r) * (1.0 / model_width)
+    for copy in sends:
+        copy.wait_send()
+
+
+def fused(gate_pre, up_pre, gate_taps, up_taps, down_weight, cotangent):
+    rows, width = gate_pre.shape
+    if rows % 16 or width % LANES or width // LANES < 8 or cotangent.shape[1] % 64:
+        return local(gate_pre, up_pre, gate_taps, up_taps, down_weight, cotangent)
+    depth = cotangent.shape[1]
+    blk = depth // lax.axis_size("rep")
+    scale = float(rows * lax.axis_size("rep") * lax.axis_size("fs")) ** (-0.5)
+    model_width = depth * lax.axis_size("fs")
+    f32, bf16 = jnp.float32, jnp.bfloat16
+    vmem = pltpu.VMEM
+    shapes = [
+        ((rows, width), bf16), ((rows, width), bf16), ((3, width), bf16), ((3, width), bf16),
+        ((width, depth), bf16), ((4 * rows, depth), bf16), ((depth, 4 * rows), bf16),
+        ((2, HALO, width), bf16), ((rows + 8, width), f32), ((rows + 8, width), f32),
+        ((rows, width), f32), ((rows, width), f32),
+        ((4, rows, width), bf16), ((4, rows, width), bf16), ((2, rows, width), bf16),
+        ((rows, width), bf16), ((rows, width), bf16),
+        ((4, blk, width), f32), ((4, blk, width), bf16), ((2, blk, width), bf16),
+        ((blk, width), bf16), ((blk, width), bf16), ((rows + 8, width), f32),
+        ((rows + 8, width), f32), ((8, width), f32), ((8, width), f32),
+        ((8, width), f32), ((4, 8, width), f32), ((8, width), f32), ((4, 8, width), f32),
+        ((1, width), f32), ((4, 1, width), f32), ((1, width), f32), ((4, 1, width), f32),
+    ]
+    outs = pl.pallas_call(
+        functools.partial(kernel, scale, model_width),
+        out_shape=[
+            jax.ShapeDtypeStruct((rows, width), bf16), jax.ShapeDtypeStruct((rows, width), bf16),
+            jax.ShapeDtypeStruct((3, width), f32), jax.ShapeDtypeStruct((3, width), f32),
+            jax.ShapeDtypeStruct((blk, width), f32), jax.ShapeDtypeStruct((1, width), f32),
+        ],
+        in_specs=[pl.BlockSpec(memory_space=pl.ANY)] * 6,
+        out_specs=[pl.BlockSpec(memory_space=pltpu.VMEM)] * 6,
+        scratch_shapes=[vmem(shape, kind) for shape, kind in shapes] + [
+            pltpu.SemaphoreType.DMA((6,)), pltpu.SemaphoreType.DMA((96,)),
+            pltpu.SemaphoreType.DMA((96,)),
+        ],
+        compiler_params=pltpu.CompilerParams(
+            collective_id=0, has_side_effects=True, vmem_limit_bytes=56 * 1024 * 1024
+        ),
+    )(gate_pre, up_pre, gate_taps, up_taps, down_weight, cotangent)
+    return outs[0], outs[1], outs[2], outs[3], outs[4][None], outs[5][0]
 
 
 def solution(mesh):
     return jax.shard_map(
-        local,
+        fused if mesh.shape["fs"] == 4 and mesh.shape["rep"] == 4 else local,
         mesh=mesh,
         in_specs=(
             P(("rep", "fs"), "tp"),

time: 200 us -> 64.9 us (0.32)
  blocking collectives: 100 us -> 0 us
  waiting for transfers between devices: 57.9 us -> 0 us
  Pallas kernels: 0 us -> 56.9 us
  between operations: 14.2 us -> 0.67 us
  other arithmetic: 10.6 us -> 1.38 us
  matrix products: 6.82 us -> 0 us
  starting transfers between devices: 6.24 us -> 0 us
  local copies, waits for them, and re-layouts: 3.38 us -> 5.71 us
    psum x1 -> x0, blocking collectives: 75.6 us -> none  [local(): norm_total, taps_total = lax.psum((norm_part, taps_part), ('rep', 'fs'))]
    pallas_call x0 -> x1, Pallas kernels: none -> 56.9 us  [fused(): pl.pallas_call(functools.partial(kernel, scale, model_width), out_shape=[...]
    all_gather x1 -> x0, waiting for transfers between devices: 34.7 us -> none  [local(): lax.all_gather(hidden, 'fs', axis=0, tiled=True)]
    all_to_all x1 -> x0, blocking collectives: 24.9 us -> none  [local(): lax.all_to_all(partial_rows, 'fs', split_axis=0, concat_axis=0, tiled=True)]
    reduce_scatter x1 -> x0, waiting for transfers between devices: 18.8 us -> none  [local(): lax.psum_scatter(folded_sum, 'rep', scatter_dimension=0, tiled=True)]
    dot_general x2 -> x0, matrix products: 6.82 us -> none  [the longest x1 4.52 us: local(): lax.dot_general(cotangent, lax.all_gather(hidden, 'fs', axis=0, tiled=Tru...]
    convert_element_type x7 -> x0, other arithmetic: 6.54 us -> none  [the longest x1 1.78 us: local(): hidden = (activated * up_conv).astype(jnp.bfloat16)]
    ppermute x2 -> x0, starting transfers between devices: 6.16 us -> none  [passed_along(): return lax.ppermute(array, axis, pairs)]
  transfers between devices with their start and end apart: 4 -> 0, of which waited for: 3 -> 0; matrix products, arithmetic and copies ran while one was open for 4% -> 0% of each run, Pallas kernels for 0% -> 0%
where the time goes in v1:
time: 64.9 us; the launch traced here: 64.7 us
  Pallas kernels  56.9 us (88%)
  local copies, waits for them, and re-layouts  5.71 us (9%)
  other arithmetic  1.38 us (2%)
  between operations  0.67 us (1%)
    pallas_call x1, Pallas kernels, fused(): pl.pallas_call(functools.partial(kernel, scale, model_width), out_shape=[...  56.9 us
    unnamed x11, local copies, waits for them, and re-layouts  5.71 us
    pallas_call x1, other arithmetic, fused(): pl.pallas_call(functools.partial(kernel, scale, model_width), out_shape=[...  1.38 us

profile of v1, /device:TPU:0, one launch (start us, length us, event | category | flops | bytes accessed | tf_op | source)
XLA Modules:
  0.0 64.7 jit_solution(15986578544411957098)
XLA Ops:
  0.6 56.9 %shard_map.109 = (bf16[160,1408]{1,0:T(8,128)(2,1)}, bf16[160,1408]{1,0:T(8,128)(2,1)}, f32[3,1408]{1,0:T(4,128)}, f32[3,1408]{1,0:T(4,128)}, f32[128,1408]{1,0:T(8,128)}, /*index=5*/f32[1,1408]{1,0:T(1,128)}) custom-call(bf16[160,1408]{1,0:T(8,128)(2,1)} %gate_hbm.1, bf16[160,1408]{1,0:T(8,128)(2,1)} %up_hbm.1, bf16[3,1408]{1,0:T(4,128)(2,1)} %gtaps_hbm.1, ...), custom_call_target="tpu_custom_call" | custom-call | tf_op jit(solution)/shard_map/pallas_call | solution.py:402
  57.6 0.0 copy-start.2
  57.6 0.0 copy-start.1
  57.6 0.0 copy-start
  57.6 1.4 %reduce = f32[1408]{0:T(1024)} reduce(f32[1,1408]{1,0:T(1,128)} %get-tuple-element.17, f32[]{:T(128)} %constant), dimensions={0}, to_apply=%get-tuple-element.17.reduce_sub_computation | reduce | bytes 11268 | tf_op jit(solution)/shard_map/pallas_call | solution.py:402
  59.0 1.8 %copy.17 = bf16[160,1408]{1,0:T(8,128)(2,1)} copy(bf16[160,1408]{1,0:T(8,128)(2,1)} %get-tuple-element.24) | data formatting | bytes 901120
  60.8 1.8 %copy.18 = bf16[160,1408]{1,0:T(8,128)(2,1)} copy(bf16[160,1408]{1,0:T(8,128)(2,1)} %get-tuple-element.25) | data formatting | bytes 901120
  62.6 0.0 copy-done.2
  62.6 0.6 copy.19
  63.2 0.0 copy-done.1
  63.2 0.6 copy.20
  63.8 0.0 copy-done
  63.8 0.9 %copy.21 = f32[1,128,1408]{2,1,0:T(8,128)} copy(f32[1,128,1408]{2,1,0:T(8,128)S(1)} %bitcast.1) | data formatting | bytes 1441792
Async XLA Ops:
  57.6 5.0 %copy-start.2 = (f32[3,1408]{1,0:T(4,128)S(1)}, f32[3,1408]{1,0:T(4,128)}, u32[]{:S(2)}) copy-start(f32[3,1408]{1,0:T(4,128)} %get-tuple-element.26) | copy-start | bytes 50692
  57.6 5.6 %copy-start.1 = (f32[3,1408]{1,0:T(4,128)S(1)}, f32[3,1408]{1,0:T(4,128)}, u32[]{:S(2)}) copy-start(f32[3,1408]{1,0:T(4,128)} %get-tuple-element.27) | copy-start | bytes 50692
  57.6 6.2 %copy-start = (f32[128,1408]{1,0:T(8,128)S(1)}, f32[128,1408]{1,0:T(8,128)}, u32[]{:S(2)}) copy-start(f32[128,1408]{1,0:T(8,128)} %get-tuple-element.16) | copy-start | bytes 2162692

commit v2 on v1

--- a/solution.py
+++ b/solution.py
@@ -99,31 +99,30 @@
 
 def column_chunks(width):
     tiles = width // LANES
-    widths = [1, 1, 2, 2]
-    rest = tiles - sum(widths)
-    if rest < 2:
-        widths, rest = [], tiles
-    widths = widths + [rest // 2, rest - rest // 2] if rest > 1 else [rest]
-    chunks, at = [], 0
-    for tiles_here in widths:
-        chunks.append((at * LANES, tiles_here * LANES))
-        at += tiles_here
-    return chunks
+    sides = (tiles - tiles // 2, tiles // 2)
+    chunks = [None] * 8
+    at = 0
+    for side, count in enumerate(sides):
+        middle = count - 2
+        for i, size in enumerate((1, middle - middle // 2, middle // 2, 1)):
+            chunks[2 * i + side] = (at * LANES, size * LANES)
+            at += size
+    return chunks, sides[0] * LANES
 
 
 def kernel(
     scale, model_width, gate_hbm, up_hbm, gtaps_hbm, utaps_hbm, weight_hbm, cot_hbm,
-    grad_gate, grad_up, gtaps_out, utaps_out, grad_down, norms_out,
-    gate, up, gtaps, utaps, weight, cot, cot_t, halo, gate_pad, up_pad, coef_gate, coef_up,
+    gg_hbm, gu_hbm, gtaps_out, utaps_out, gd_hbm, norms_out,
+    gate, up, gtaps, utaps, weight, cot, cot_t, halo_out, halo, gate_pad, up_pad, coef_gate, coef_up,
     hid, parts, rs1, rs2, rs_out, prod, prod_out, zs1, zs2, z_out, dg_pad, du_pad,
     dhalo_out, dhalo_in, taps_out1, taps_in1, taps_out2, taps_in2,
-    norm_out1, norm_in1, norm_out2, norm_in2, load_sem, send_sem, recv_sem,
+    norm_out1, norm_in1, norm_out2, norm_in2, grad_gate, grad_up, grad_down, load_sem, store_sem, send_sem, recv_sem,
 ):
     f = lax.axis_index("fs")
     r = lax.axis_index("rep")
     rows, width = gate.shape
     blk = grad_down.shape[0]
-    chunks = column_chunks(width)
+    chunks, split = column_chunks(width)
     n = len(chunks)
     sends = []
 
@@ -140,7 +139,6 @@
     for d in (1, 2, 3):
         pl.semaphore_signal(barrier, inc=1, device_id={"fs": (f + d) % 4}, device_id_type=MESH)
         pl.semaphore_signal(barrier, inc=1, device_id={"rep": (r + d) % 4}, device_id_type=MESH)
-    pl.semaphore_wait(barrier, 6)
 
     def push(src, dst, axis, to):
         k = len(sends)
@@ -158,14 +156,6 @@
     def tile_list(c):
         return [pl.ds(at, LANES) for at in range(chunks[c][0], chunks[c][0] + chunks[c][1], LANES)]
 
-    loads[0].wait()
-    loads[1].wait()
-    nxt = (f + 1) % 4
-    halo_in = [
-        push(gate.at[pl.ds(rows - HALO, HALO)], halo.at[0], "fs", nxt),
-        push(up.at[pl.ds(rows - HALO, HALO)], halo.at[1], "fs", nxt),
-    ]
-
     def part(c):
         product = lax.dot_general(
             cot[...], weight[cols(c), :], (((1,), (1,)), ((), ())),
@@ -193,27 +183,47 @@
             ).astype(jnp.bfloat16)
         rs2_in[c] = push(rs_out.at[:, cols(c)], rs2.at[:, cols(c)], "fs", to)
 
-    def hidden(c):
-        for t in tile_list(c):
-            gc = [gtaps[k : k + 1, t].astype(jnp.float32) for k in range(3)]
-            uc = [utaps[k : k + 1, t].astype(jnp.float32) for k in range(3)]
-            g_conv = sum(gc[k] * gate_pad[pl.ds(6 + k, rows), t] for k in range(3))
-            u_conv = sum(uc[k] * up_pad[pl.ds(6 + k, rows), t] for k in range(3))
-            sig = jax.nn.sigmoid(g_conv)
-            act = g_conv * sig
-            hid[f, :, t] = (act * u_conv).astype(jnp.bfloat16)
-            coef_up[:, t] = act
-            coef_gate[:, t] = u_conv * sig * (1.0 + g_conv * (1.0 - sig))
-        m1, m2 = FS_MASKS[c % 2]
-        ag1_in[c] = push(hid.at[f, :, cols(c)], hid.at[f, :, cols(c)], "fs", flip(f, m1))
+    def activate(t, top, count):
+        gc = [gtaps[k : k + 1, t].astype(jnp.float32) for k in range(3)]
+        uc = [utaps[k : k + 1, t].astype(jnp.float32) for k in range(3)]
+        g_conv = sum(gc[k] * gate_pad[pl.ds(top + 6 + k, count), t] for k in range(3))
+        u_conv = sum(uc[k] * up_pad[pl.ds(top + 6 + k, count), t] for k in range(3))
+        sig = jax.nn.sigmoid(g_conv)
+        act = g_conv * sig
+        at = pl.ds(top, count)
+        hid[f, at, t] = (act * u_conv).astype(jnp.bfloat16)
+        coef_up[at, t] = act
+        coef_gate[at, t] = u_conv * sig * (1.0 + g_conv * (1.0 - sig))
+
+    lower = pl.ds(HALO, rows - HALO)
+
+    def pass_on(slot, row_range, col_range, to):
+        ref = hid.at[slot, row_range, col_range]
+        return push(ref, ref, "fs", to)
+
+    def ag_first(c):
+        ag1_in[c] = pass_on(f, lower, cols(c), flip(f, FS_MASKS[c % 2][0]))
 
     def ag_second(c):
         m1, m2 = FS_MASKS[c % 2]
         to = flip(f, m2)
-        own = push(hid.at[f, :, cols(c)], hid.at[f, :, cols(c)], "fs", to)
+        own = pass_on(f, lower, cols(c), to)
         ag1_in[c].wait_recv()
-        slot = flip(f, m1)
-        ag2_in[c] = [own, push(hid.at[slot, :, cols(c)], hid.at[slot, :, cols(c)], "fs", to)]
+        ag2_in[c] = [own, pass_on(flip(f, m1), lower, cols(c), to)]
+
+    upper = pl.ds(0, HALO)
+    side_cols = (pl.ds(0, split), pl.ds(split, width - split))
+
+    def top_first():
+        return [pass_on(f, upper, side_cols[i], flip(f, FS_MASKS[i][0])) for i in range(2)]
+
+    def top_second(first):
+        out = []
+        for i, (m1, m2) in enumerate(FS_MASKS):
+            out.append(pass_on(f, upper, side_cols[i], flip(f, m2)))
+            first[i].wait_recv()
+            out.append(pass_on(flip(f, m1), upper, side_cols[i], flip(f, m2)))
+        return out
 
     def product(c):
         for copy in ag2_in[c]:
@@ -281,55 +291,77 @@
         landing[me] = own[...]
         return (landing[0] + landing[1]) + (landing[2] + landing[3])
 
+    for i in (0, 1, 4, 5):
+        loads[i].wait()
+    gate_pad[pl.ds(8, rows), :] = gate[...].astype(jnp.float32)
+    up_pad[pl.ds(8, rows), :] = up[...].astype(jnp.float32)
+    halo_out[0:2, :] = gate_pad[rows + 6 : rows + 8, :].astype(jnp.bfloat16)
+    halo_out[2:4, :] = up_pad[rows + 6 : rows + 8, :].astype(jnp.bfloat16)
+    taps_out1[...] = jnp.zeros_like(taps_out1)
+    dhalo_out[...] = jnp.zeros_like(dhalo_out)
+    for c in range(n):
+        for t in tile_list(c):
+            activate(t, HALO, rows - HALO)
+    pl.semaphore_wait(barrier, 6)
+    halo_in = push(halo_out, halo, "fs", (f + 1) % 4)
+    ag_first(0)
+    ag_first(1)
+    ag_first(2)
+    ag_first(3)
     loads[2].wait()
     loads[3].wait()
     part(0)
-    rs_first(0)
     part(1)
-    rs_first(1)
-    gate_pad[pl.ds(8, rows), :] = gate[...].astype(jnp.float32)
-    up_pad[pl.ds(8, rows), :] = up[...].astype(jnp.float32)
-    taps_out1[...] = jnp.zeros_like(taps_out1)
-    dhalo_out[...] = jnp.zeros_like(dhalo_out)
-    loads[4].wait()
-    loads[5].wait()
-    for copy in halo_in:
-        copy.wait_recv()
-    inner = (f > 0).astype(jnp.float32)
-    gate_pad[6:8, :] = halo[0].astype(jnp.float32)[HALO - 2 :] * inner
-    up_pad[6:8, :] = halo[1].astype(jnp.float32)[HALO - 2 :] * inner
-
-    hidden(0)
-    hidden(1)
-    hidden(2)
-    hidden(3)
+    halo_in.wait_recv()
+    edge = halo[...].astype(jnp.float32) * (f > 0).astype(jnp.float32)
+    gate_pad[6:8, :] = edge[0:2]
+    up_pad[6:8, :] = edge[2:4]
+    for c in range(n):
+        for t in tile_list(c):
+            activate(t, 0, HALO)
+    top1 = top_first()
+    ag_first(4)
+    ag_first(5)
     ag_second(0)
     ag_second(1)
+    ag_first(6)
+    ag_first(7)
+    top2 = top_second(top1)
     cot_t[...] = cot[...].T
-    hidden(4)
-    hidden(5)
+    rs_first(0)
+    rs_first(1)
     ag_second(2)
     ag_second(3)
     part(2)
     part(3)
+    for copy in top2:
+        copy.wait_recv()
     product(0)
     product(1)
     ag_second(4)
     ag_second(5)
+    ag_second(6)
+    ag_second(7)
     rs_first(2)
     rs_first(3)
     part(4)
     part(5)
+    rs_first(4)
+    rs_first(5)
     product(2)
     product(3)
+    part(6)
+    part(7)
+    rs_first(6)
+    rs_first(7)
     z_second(0)
     z_second(1)
     rs_second(0)
     rs_second(1)
-    rs_first(4)
-    rs_first(5)
     product(4)
     product(5)
+    product(6)
+    product(7)
     z_second(2)
     z_second(3)
     rs_second(2)
@@ -338,20 +370,30 @@
     z_last(1)
     rs_last(0)
     rs_last(1)
+    z_second(4)
+    z_second(5)
     rs_second(4)
     rs_second(5)
+    z_last(2)
+    z_last(3)
     rs_last(2)
     rs_last(3)
-    z_second(4)
-    z_second(5)
-    z_last(2)
-    z_last(3)
+    z_second(6)
+    z_second(7)
+    rs_second(6)
+    rs_second(7)
+    z_last(4)
+    z_last(5)
     rs_last(4)
     rs_last(5)
+    rs_last(6)
+    rs_last(7)
     taps1 = spread(taps_out1, taps_in1, "fs", f)
     dhalo = push(dhalo_out, dhalo_in, "fs", (f + 3) % 4)
-    z_last(4)
-    z_last(5)
+    z_last(6)
+    z_last(7)
+    store_down = pltpu.make_async_copy(grad_down, gd_hbm, store_sem.at[0])
+    store_down.start()
     norm1 = spread(norm_out1, norm_in1, "fs", f)
     taps_out2[...] = gather_sum(taps1, taps_out1, taps_in1, f)
     taps2 = spread(taps_out2, taps_in2, "rep", r)
@@ -368,12 +410,34 @@
                     taps[2 - k : 3 - k, t].astype(jnp.float32) * pad[pl.ds(k, rows), t]
                     for k in range(3)
                 ).astype(jnp.bfloat16)
+    stores = [store_down]
+    for i, (src, dst) in enumerate(((grad_gate, gg_hbm), (grad_up, gu_hbm))):
+        stores.append(pltpu.make_async_copy(src, dst, store_sem.at[1 + i]))
+        stores[-1].start()
     taps_total = gather_sum(taps2, taps_out2, taps_in2, r) * scale
     gtaps_out[...] = taps_total[0:3]
     utaps_out[...] = taps_total[3:6]
     norms_out[...] = gather_sum(norm2, norm_out2, norm_in2, r) * (1.0 / model_width)
+    for copy in stores:
+        copy.wait()
     for copy in sends:
         copy.wait_send()
+
+
+def hand_over(*refs):
+    ins, outs, held, sems_in, sems_out = refs[:6], refs[6:12], refs[12:18], refs[18], refs[19]
+    order = (4, 0, 1, 2, 3)
+    fetch = {i: pltpu.make_async_copy(ins[i], held[i], sems_in.at[i]) for i in range(6)}
+    store = {i: pltpu.make_async_copy(held[i], outs[i], sems_out.at[i]) for i in order}
+    for i in (5,) + order:
+        fetch[i].start()
+    fetch[5].wait()
+    outs[5][...] = held[5][0]
+    for i in order:
+        fetch[i].wait()
+        store[i].start()
+    for i in order:
+        store[i].wait()
 
 
 def fused(gate_pre, up_pre, gate_taps, up_taps, down_weight, cotangent):
@@ -389,7 +453,7 @@
     shapes = [
         ((rows, width), bf16), ((rows, width), bf16), ((3, width), bf16), ((3, width), bf16),
         ((width, depth), bf16), ((4 * rows, depth), bf16), ((depth, 4 * rows), bf16),
-        ((2, HALO, width), bf16), ((rows + 8, width), f32), ((rows + 8, width), f32),
+        ((4, width), bf16), ((4, width), bf16), ((rows + 8, width), f32), ((rows + 8, width), f32),
         ((rows, width), f32), ((rows, width), f32),
         ((4, rows, width), bf16), ((4, rows, width), bf16), ((2, rows, width), bf16),
         ((rows, width), bf16), ((rows, width), bf16),
@@ -398,6 +462,7 @@
         ((rows + 8, width), f32), ((8, width), f32), ((8, width), f32),
         ((8, width), f32), ((4, 8, width), f32), ((8, width), f32), ((4, 8, width), f32),
         ((1, width), f32), ((4, 1, width), f32), ((1, width), f32), ((4, 1, width), f32),
+        ((rows, width), bf16), ((rows, width), bf16), ((blk, width), f32),
     ]
     outs = pl.pallas_call(
         functools.partial(kernel, scale, model_width),
@@ -407,16 +472,29 @@
             jax.ShapeDtypeStruct((blk, width), f32), jax.ShapeDtypeStruct((1, width), f32),
         ],
         in_specs=[pl.BlockSpec(memory_space=pl.ANY)] * 6,
-        out_specs=[pl.BlockSpec(memory_space=pltpu.VMEM)] * 6,
+        out_specs=[
+            pl.BlockSpec(memory_space=pl.ANY if i in (0, 1, 4) else pltpu.VMEM) for i in range(6)
+        ],
         scratch_shapes=[vmem(shape, kind) for shape, kind in shapes] + [
-            pltpu.SemaphoreType.DMA((6,)), pltpu.SemaphoreType.DMA((96,)),
+            pltpu.SemaphoreType.DMA((6,)), pltpu.SemaphoreType.DMA((3,)),
+            pltpu.SemaphoreType.DMA((96,)),
             pltpu.SemaphoreType.DMA((96,)),
         ],
         compiler_params=pltpu.CompilerParams(
             collective_id=0, has_side_effects=True, vmem_limit_bytes=56 * 1024 * 1024
         ),
     )(gate_pre, up_pre, gate_taps, up_taps, down_weight, cotangent)
-    return outs[0], outs[1], outs[2], outs[3], outs[4][None], outs[5][0]
+    final = pl.pallas_call(
+        hand_over,
+        out_shape=[jax.ShapeDtypeStruct(x.shape, x.dtype) for x in outs[:5]]
+        + [jax.ShapeDtypeStruct((width,), f32)],
+        in_specs=[pl.BlockSpec(memory_space=pl.ANY)] * 6,
+        out_specs=[pl.BlockSpec(memory_space=pl.ANY)] * 5 + [pl.BlockSpec(memory_space=pltpu.VMEM)],
+        scratch_shapes=[vmem(x.shape, x.dtype) for x in outs]
+        + [pltpu.SemaphoreType.DMA((6,)), pltpu.SemaphoreType.DMA((6,))],
+        compiler_params=pltpu.CompilerParams(vmem_limit_bytes=56 * 1024 * 1024),
+    )(*outs)
+    return final[0], final[1], final[2], final[3], final[4][None], final[5]
 
 
 def solution(mesh):

time: 64.9 us -> 59.7 us (0.920)
  local copies, waits for them, and re-layouts: 5.71 us -> 0 us
  Pallas kernels: 56.9 us -> 58.8 us
  other arithmetic: 1.38 us -> 0 us
    unnamed x11 -> x0, local copies, waits for them, and re-layouts: 5.71 us -> none
    pallas_call x0 -> x1, Pallas kernels: none -> 2.98 us  [fused(): pl.pallas_call(hand_over, out_shape=[jax.ShapeDtypeStruct(x.shape, x.dtyp...]
    pallas_call x1 -> x0, other arithmetic: 1.38 us -> none  [fused(): pl.pallas_call(functools.partial(kernel, scale, model_width), out_shape=[...]
    pallas_call x1, Pallas kernels: 56.9 us -> 55.8 us  [fused(): pl.pallas_call(functools.partial(kernel, scale, model_width), out_shape=[...]
where the time goes in v2:
time: 59.7 us; the launch traced here: 59.5 us
  Pallas kernels  58.8 us (98%)
  between operations  0.64 us (1%)
    pallas_call x1, Pallas kernels, fused(): pl.pallas_call(functools.partial(kernel, scale, model_width), out_shape=[...  55.8 us
    pallas_call x1, Pallas kernels, fused(): pl.pallas_call(hand_over, out_shape=[jax.ShapeDtypeStruct(x.shape, x.dtyp...  2.98 us

profile of v2, /device:TPU:0, one launch (start us, length us, event | category | flops | bytes accessed | tf_op | source)
XLA Modules:
  0.0 59.5 jit_solution(16977714185041971474)
XLA Ops:
  0.6 55.8 %shard_map.109 = (bf16[160,1408]{1,0:T(8,128)(2,1)}, bf16[160,1408]{1,0:T(8,128)(2,1)}, f32[3,1408]{1,0:T(4,128)}, f32[3,1408]{1,0:T(4,128)}, f32[128,1408]{1,0:T(8,128)}, /*index=5*/f32[1,1408]{1,0:T(1,128)}) custom-call(bf16[160,1408]{1,0:T(8,128)(2,1)} %gate_hbm.1, bf16[160,1408]{1,0:T(8,128)(2,1)} %up_hbm.1, bf16[3,1408]{1,0:T(4,128)(2,1)} %gtaps_hbm.1, ...), custom_call_target="tpu_custom_call" | custom-call | tf_op jit(solution)/shard_map/pallas_call | solution.py:467
  56.5 3.0 %shard_map.110 = (bf16[160,1408]{1,0:T(8,128)(2,1)}, bf16[160,1408]{1,0:T(8,128)(2,1)}, f32[3,1408]{1,0:T(4,128)}, f32[3,1408]{1,0:T(4,128)}, f32[128,1408]{1,0:T(8,128)}, /*index=5*/f32[1408]{0:T(1024)}) custom-call(bf16[160,1408]{1,0:T(8,128)(2,1)} %get-tuple-element.18.refs_0_, bf16[160,1408]{1,0:T(8,128)(2,1)} %get-tuple-element.19.refs_1_, ...), custom_call_target="tpu_custom_call" | custom-call | tf_op jit(solution)/shard_map/pallas_call | solution.py:487

commit v3 on v2

--- a/solution.py
+++ b/solution.py
@@ -113,7 +113,7 @@
 def kernel(
     scale, model_width, gate_hbm, up_hbm, gtaps_hbm, utaps_hbm, weight_hbm, cot_hbm,
     gg_hbm, gu_hbm, gtaps_out, utaps_out, gd_hbm, norms_out,
-    gate, up, gtaps, utaps, weight, cot, cot_t, halo_out, halo, gate_pad, up_pad, coef_gate, coef_up,
+    gate, up, gtaps, utaps, weight, cot, cot_t, edge, edges, edge_pad, patch, gate_pad, up_pad, coef_gate, coef_up,
     hid, parts, rs1, rs2, rs_out, prod, prod_out, zs1, zs2, z_out, dg_pad, du_pad,
     dhalo_out, dhalo_in, taps_out1, taps_in1, taps_out2, taps_in2,
     norm_out1, norm_in1, norm_out2, norm_in2, grad_gate, grad_up, grad_down, load_sem, store_sem, send_sem, recv_sem,
@@ -183,53 +183,70 @@
             ).astype(jnp.bfloat16)
         rs2_in[c] = push(rs_out.at[:, cols(c)], rs2.at[:, cols(c)], "fs", to)
 
-    def activate(t, top, count):
+    def activation(t, top, count):
         gc = [gtaps[k : k + 1, t].astype(jnp.float32) for k in range(3)]
         uc = [utaps[k : k + 1, t].astype(jnp.float32) for k in range(3)]
         g_conv = sum(gc[k] * gate_pad[pl.ds(top + 6 + k, count), t] for k in range(3))
         u_conv = sum(uc[k] * up_pad[pl.ds(top + 6 + k, count), t] for k in range(3))
         sig = jax.nn.sigmoid(g_conv)
         act = g_conv * sig
-        at = pl.ds(top, count)
-        hid[f, at, t] = (act * u_conv).astype(jnp.bfloat16)
-        coef_up[at, t] = act
-        coef_gate[at, t] = u_conv * sig * (1.0 + g_conv * (1.0 - sig))
-
-    lower = pl.ds(HALO, rows - HALO)
-
-    def pass_on(slot, row_range, col_range, to):
-        ref = hid.at[slot, row_range, col_range]
+        return act, u_conv * sig * (1.0 + g_conv * (1.0 - sig)), act * u_conv
+
+    def activate(t):
+        act, slope, rows_out = activation(t, 0, rows)
+        row = lax.broadcasted_iota(jnp.int32, rows_out.shape, 0)
+        hid[f, :, t] = jnp.where(row < 2, 0.0, rows_out).astype(jnp.bfloat16)
+        coef_up[:, t] = act
+        coef_gate[:, t] = slope
+
+    def pass_on(slot, c, to):
+        ref = hid.at[slot, :, cols(c)]
         return push(ref, ref, "fs", to)
 
     def ag_first(c):
-        ag1_in[c] = pass_on(f, lower, cols(c), flip(f, FS_MASKS[c % 2][0]))
+        ag1_in[c] = pass_on(f, c, flip(f, FS_MASKS[c % 2][0]))
 
     def ag_second(c):
         m1, m2 = FS_MASKS[c % 2]
         to = flip(f, m2)
-        own = pass_on(f, lower, cols(c), to)
+        own = pass_on(f, c, to)
         ag1_in[c].wait_recv()
-        ag2_in[c] = [own, pass_on(flip(f, m1), lower, cols(c), to)]
-
-    upper = pl.ds(0, HALO)
-    side_cols = (pl.ds(0, split), pl.ds(split, width - split))
-
-    def top_first():
-        return [pass_on(f, upper, side_cols[i], flip(f, FS_MASKS[i][0])) for i in range(2)]
-
-    def top_second(first):
-        out = []
-        for i, (m1, m2) in enumerate(FS_MASKS):
-            out.append(pass_on(f, upper, side_cols[i], flip(f, m2)))
-            first[i].wait_recv()
-            out.append(pass_on(flip(f, m1), upper, side_cols[i], flip(f, m2)))
-        return out
+        ag2_in[c] = [own, pass_on(flip(f, m1), c, to)]
+
+    def edge_rows(incoming):
+        for copy in incoming:
+            copy.wait_recv()
+        edges[f] = edge[...]
+        patch[...] = jnp.zeros_like(patch)
+        for slot in range(4):
+            here = edges[slot].astype(jnp.float32)
+            before = edges[slot - 1].astype(jnp.float32) if slot else jnp.zeros_like(here)
+            for i in range(2):
+                edge_pad[i, slot, 0:2, :] = before[4 + 2 * i : 6 + 2 * i]
+                edge_pad[i, slot, 2:4, :] = here[2 * i : 2 * i + 2]
+        for c in range(n):
+            for t in tile_list(c):
+                gc = [gtaps[k : k + 1, t].astype(jnp.float32) for k in range(3)]
+                uc = [utaps[k : k + 1, t].astype(jnp.float32) for k in range(3)]
+                g_conv = sum(gc[k] * edge_pad[0, :, k : k + 2, t] for k in range(3))
+                u_conv = sum(uc[k] * edge_pad[1, :, k : k + 2, t] for k in range(3))
+                patch[:, 0:2, t] = (g_conv * jax.nn.sigmoid(g_conv) * u_conv).astype(jnp.bfloat16)
+        gate_pad[6:8, :] = edge_pad[0, f, 0:2, :]
+        up_pad[6:8, :] = edge_pad[1, f, 0:2, :]
+        for c in range(n):
+            for t in tile_list(c):
+                act, slope, _ = activation(t, 0, 8)
+                coef_up[0:8, t] = act
+                coef_gate[0:8, t] = slope
 
     def product(c):
         for copy in ag2_in[c]:
             copy.wait_recv()
+        block = jnp.concatenate(
+            [hid[:, 0:HALO, cols(c)] + patch[:, :, cols(c)], hid[:, HALO:, cols(c)]], axis=1
+        )
         result = jnp.dot(
-            cot_t[...], hid[:, :, cols(c)].reshape(4 * rows, chunks[c][1]),
+            cot_t[...], block.reshape(4 * rows, chunks[c][1]),
             preferred_element_type=jnp.float32,
         ).reshape(4, blk, chunks[c][1])
         prod[:, :, cols(c)] = result
@@ -295,97 +312,90 @@
         loads[i].wait()
     gate_pad[pl.ds(8, rows), :] = gate[...].astype(jnp.float32)
     up_pad[pl.ds(8, rows), :] = up[...].astype(jnp.float32)
-    halo_out[0:2, :] = gate_pad[rows + 6 : rows + 8, :].astype(jnp.bfloat16)
-    halo_out[2:4, :] = up_pad[rows + 6 : rows + 8, :].astype(jnp.bfloat16)
+    gate_pad[0:8, :] = jnp.zeros((8, width), jnp.float32)
+    up_pad[0:8, :] = jnp.zeros((8, width), jnp.float32)
+    for i, pad in enumerate((gate_pad, up_pad)):
+        edge[2 * i : 2 * i + 2, :] = pad[8:10, :].astype(jnp.bfloat16)
+        edge[4 + 2 * i : 6 + 2 * i, :] = pad[rows + 6 : rows + 8, :].astype(jnp.bfloat16)
     taps_out1[...] = jnp.zeros_like(taps_out1)
     dhalo_out[...] = jnp.zeros_like(dhalo_out)
     for c in range(n):
         for t in tile_list(c):
-            activate(t, HALO, rows - HALO)
+            activate(t)
     pl.semaphore_wait(barrier, 6)
-    halo_in = push(halo_out, halo, "fs", (f + 1) % 4)
     ag_first(0)
     ag_first(1)
+    edge_in = spread(edge, edges, "fs", f)
     ag_first(2)
     ag_first(3)
     loads[2].wait()
     loads[3].wait()
+    cot_t[...] = cot[...].T
     part(0)
     part(1)
-    halo_in.wait_recv()
-    edge = halo[...].astype(jnp.float32) * (f > 0).astype(jnp.float32)
-    gate_pad[6:8, :] = edge[0:2]
-    up_pad[6:8, :] = edge[2:4]
-    for c in range(n):
-        for t in tile_list(c):
-            activate(t, 0, HALO)
-    top1 = top_first()
+    ag_second(0)
+    ag_second(1)
     ag_first(4)
     ag_first(5)
-    ag_second(0)
-    ag_second(1)
+    edge_rows(edge_in)
+    part(2)
+    part(3)
+    ag_second(2)
+    ag_second(3)
     ag_first(6)
     ag_first(7)
-    top2 = top_second(top1)
-    cot_t[...] = cot[...].T
-    rs_first(0)
-    rs_first(1)
-    ag_second(2)
-    ag_second(3)
-    part(2)
-    part(3)
-    for copy in top2:
-        copy.wait_recv()
     product(0)
     product(1)
     ag_second(4)
     ag_second(5)
+    rs_first(0)
+    rs_first(1)
+    part(4)
+    part(5)
+    product(2)
+    product(3)
     ag_second(6)
     ag_second(7)
+    z_second(0)
+    z_second(1)
     rs_first(2)
     rs_first(3)
-    part(4)
-    part(5)
     rs_first(4)
     rs_first(5)
-    product(2)
-    product(3)
     part(6)
     part(7)
     rs_first(6)
     rs_first(7)
-    z_second(0)
-    z_second(1)
+    product(4)
+    product(5)
     rs_second(0)
     rs_second(1)
-    product(4)
-    product(5)
     product(6)
     product(7)
     z_second(2)
     z_second(3)
+    z_last(0)
+    z_last(1)
     rs_second(2)
     rs_second(3)
-    z_last(0)
-    z_last(1)
-    rs_last(0)
-    rs_last(1)
     z_second(4)
     z_second(5)
     rs_second(4)
     rs_second(5)
-    z_last(2)
-    z_last(3)
-    rs_last(2)
-    rs_last(3)
     z_second(6)
     z_second(7)
     rs_second(6)
     rs_second(7)
+    rs_last(0)
+    rs_last(1)
+    rs_last(2)
+    rs_last(3)
+    z_last(2)
+    z_last(3)
+    rs_last(4)
+    rs_last(5)
     z_last(4)
     z_last(5)
-    rs_last(4)
-    rs_last(5)
     rs_last(6)
     rs_last(7)
     taps1 = spread(taps_out1, taps_in1, "fs", f)
@@ -453,7 +463,8 @@
     shapes = [
         ((rows, width), bf16), ((rows, width), bf16), ((3, width), bf16), ((3, width), bf16),
         ((width, depth), bf16), ((4 * rows, depth), bf16), ((depth, 4 * rows), bf16),
-        ((4, width), bf16), ((4, width), bf16), ((rows + 8, width), f32), ((rows + 8, width), f32),
+        ((8, width), bf16), ((4, 8, width), bf16),
+        ((2, 4, 8, width), f32), ((4, HALO, width), bf16), ((rows + 8, width), f32), ((rows + 8, width), f32),
         ((rows, width), f32), ((rows, width), f32),
         ((4, rows, width), bf16), ((4, rows, width), bf16), ((2, rows, width), bf16),
         ((rows, width), bf16), ((rows, width), bf16),

time: 59.7 us -> 57.3 us (0.960)
  Pallas kernels: 58.8 us -> 56.3 us
    pallas_call x1, Pallas kernels: 55.8 us -> 53.4 us  [fused(): pl.pallas_call(functools.partial(kernel, scale, model_width), out_shape=[...]
where the time goes in v3:
time: 57.3 us; the launch traced here: 57 us
  Pallas kernels  56.3 us (98%)
  between operations  0.64 us (1%)
    pallas_call x1, Pallas kernels, fused(): pl.pallas_call(functools.partial(kernel, scale, model_width), out_shape=[...  53.4 us
    pallas_call x1, Pallas kernels, fused(): pl.pallas_call(hand_over, out_shape=[jax.ShapeDtypeStruct(x.shape, x.dtyp...  2.98 us

profile of v3, /device:TPU:0, one launch (start us, length us, event | category | flops | bytes accessed | tf_op | source)
XLA Modules:
  0.0 57.0 jit_solution(4546678907208644191)
XLA Ops:
  0.6 53.4 %shard_map.109 = (bf16[160,1408]{1,0:T(8,128)(2,1)}, bf16[160,1408]{1,0:T(8,128)(2,1)}, f32[3,1408]{1,0:T(4,128)}, f32[3,1408]{1,0:T(4,128)}, f32[128,1408]{1,0:T(8,128)}, /*index=5*/f32[1,1408]{1,0:T(1,128)}) custom-call(bf16[160,1408]{1,0:T(8,128)(2,1)} %gate_hbm.1, bf16[160,1408]{1,0:T(8,128)(2,1)} %up_hbm.1, bf16[3,1408]{1,0:T(4,128)(2,1)} %gtaps_hbm.1, ...), custom_call_target="tpu_custom_call" | custom-call | tf_op jit(solution)/shard_map/pallas_call | solution.py:478
  54.0 3.0 %shard_map.110 = (bf16[160,1408]{1,0:T(8,128)(2,1)}, bf16[160,1408]{1,0:T(8,128)(2,1)}, f32[3,1408]{1,0:T(4,128)}, f32[3,1408]{1,0:T(4,128)}, f32[128,1408]{1,0:T(8,128)}, /*index=5*/f32[1408]{0:T(1024)}) custom-call(bf16[160,1408]{1,0:T(8,128)(2,1)} %get-tuple-element.18.refs_0_, bf16[160,1408]{1,0:T(8,128)(2,1)} %get-tuple-element.19.refs_1_, ...), custom_call_target="tpu_custom_call" | custom-call | tf_op jit(solution)/shard_map/pallas_call | solution.py:498
